TPU v7x, 32 devices: a whole 2x2x4 slice. The times are simulated.
32 devices in a mesh: sp: 8 (over z, x), tp: 4 (over y, core).
Axes of the slice: x: 2, y: 2, z: 4, core: 2. Of those that a mesh axis runs over, the one named last changes fastest.
Arguments:
- stream: bfloat16 [4096, 2048], P('sp', 'tp'), may hold values from -6 to 6
- norm_gain: float32 [2, 2048], replicated, may hold values from 0.1 to 1.9
- w_value: bfloat16 [2, 2048, 2048], P(None, 'sp', 'tp'), may hold values from -0.125 to 0.125
- w_inner: bfloat16 [2, 2048, 2048], P(None, 'sp', 'tp'), may hold values from -0.125 to 0.125
- w_outer: bfloat16 [2, 2048, 2048], P(None, 'sp', 'tp'), may hold values from -0.125 to 0.125
- conv_taps: float32 [2, 3, 2048], P(None, None, 'tp'), may hold values from -3 to 3
- w_output: bfloat16 [2, 2048, 2048], P(None, 'tp', 'sp'), may hold values from -0.125 to 0.125
Outputs:
- result: bfloat16 [4096, 2048], P('sp', 'tp')
All inputs are finite; a program needn't handle non-finite values.
Results may differ from a plain program's by a relative error of at most 0.02.
Values may be sent and summed in bfloat16 or wider, within the bound.
A program may use at most 64 MiB of HBM per device.

v0:
```python
import jax
import jax.numpy as jnp
from jax import lax
from jax.sharding import PartitionSpec as P

LAYERS = 2


EPSILON = 1e-06


def passed_along(block, axis, distance):
    devices = range(lax.axis_size(axis))
    route = [(i - distance, i) for i in devices if i - distance in devices]
    return lax.ppermute(block, axis, route)


def on_device(stream, norm_gain, w_value, w_inner, w_outer, conv_taps, w_output):
    gathered_in = (
        lax.all_gather(w_value, "sp", axis=1, tiled=True),
        lax.all_gather(w_inner, "sp", axis=1, tiled=True),
        lax.all_gather(w_outer, "sp", axis=1, tiled=True),
    )
    gathered_out = lax.all_gather(w_output, "sp", axis=2, tiled=True)
    stream_now = stream
    for layer_index in range(LAYERS):
        layer_value = gathered_in[0][layer_index]
        layer_inner = gathered_in[1][layer_index]
        layer_outer = gathered_in[2][layer_index]
        layer_output = gathered_out[layer_index]
        full_rows = lax.all_gather(stream_now, "tp", axis=1, tiled=True)
        row_float = full_rows.astype(jnp.float32)
        scale = lax.rsqrt(jnp.mean(row_float * row_float, axis=-1, keepdims=True) + EPSILON)
        normed = (row_float * scale * norm_gain[layer_index]).astype(jnp.bfloat16)
        row_count = normed.shape[0]
        value_proj = jnp.dot(normed, layer_value, preferred_element_type=jnp.float32)
        inner_gate = jnp.dot(normed, layer_inner, preferred_element_type=jnp.float32)
        outer_gate = jnp.dot(normed, layer_outer, preferred_element_type=jnp.float32)
        mixed = (inner_gate * value_proj).astype(jnp.bfloat16)
        before = passed_along(mixed[row_count - 2 :], "sp", 1)
        padded = jnp.concatenate([before, mixed], axis=0).astype(jnp.float32)
        taps = conv_taps[layer_index]
        convolved = (
            taps[0] * padded[0:row_count]
            + taps[1] * padded[1 : row_count + 1]
            + taps[2] * padded[2:]
        )
        gated = (outer_gate * convolved).astype(jnp.bfloat16)
        terms = jnp.dot(gated, layer_output, preferred_element_type=jnp.float32).astype(
            jnp.bfloat16
        )
        summed = lax.psum_scatter(
            terms.astype(jnp.float32).astype(jnp.bfloat16), "tp", scatter_dimension=1, tiled=True
        ).astype(jnp.float32)
        stream_now = (stream_now.astype(jnp.float32) + summed).astype(jnp.bfloat16)
    return stream_now


def solution(mesh):
    in_specs = (
        P("sp", "tp"),
        P(),
        P(None, "sp", "tp"),
        P(None, "sp", "tp"),
        P(None, "sp", "tp"),
        P(None, None, "tp"),
        P(None, "tp", "sp"),
    )
    out_specs = P("sp", "tp")
    return jax.shard_map(
        on_device, mesh=mesh, in_specs=in_specs, out_specs=out_specs, check_vma=False
    )
```

profile of v0, /device:TPU:26, one launch (start us, length us, event | category | flops | bytes accessed | tf_op | source)
XLA Modules:
  0.0 448.4 jit_solution(300876081806969072)
XLA Ops:
  6.5 0.0 all-gather.7.cloned.1.call-start
  6.5 0.7 all-gather.7.cloned.1.call-update
  7.3 0.0 all-gather.13.cloned.1.call-start
  7.3 0.7 all-gather.13.cloned.1.call-update
  8.0 0.0 all-gather.11.cloned.1.call-start
  8.1 0.7 all-gather.11.cloned.1.call-update
  8.7 0.0 all-gather.9.cloned.1.call-start
  8.8 0.5 all-gather.9.cloned.1.call-update
  9.3 0.0 all-gather.15.cloned.1.call-start
  9.4 0.5 all-gather.15.cloned.1.call-update
  9.9 0.0 reduce-scatter.3.cloned.1.call-start
  10.0 0.0 copy-done.4
  10.0 22.5 %all-gather.7.cloned.1.call-done = bf16[512,2048]{1,0:T(8,128)(2,1)} async-done(((bf16[512,512]{1,0:T(8,128)(2,1)}), bf16[512,2048]{1,0:T(8,128)(2,1)}) %all-gather.7.cloned.1.call-update) | async-done | bytes 2097168 | tf_op jit(solution)/shard_map/all_gather | solution.py:31
  32.4 2.2 fusion
  34.7 70.4 %all-gather.13.cloned.1.call-done = bf16[2,2048,512]{2,1,0:T(8,128)(2,1)} async-done(((bf16[2,256,512]{2,1,0:T(8,128)(2,1)}), bf16[2,2048,512]{2,1,0:T(8,128)(2,1)}) %all-gather.13.cloned.1.call-update) | async-done | bytes 4194320 | tf_op jit(solution)/shard_map/all_gather | solution.py:20
  105.0 0.0 copy-done.2
  105.1 2.9 fusion.9
  107.9 0.0 copy-start.5
  108.0 70.6 %all-gather.11.cloned.1.call-done = bf16[2,2048,512]{2,1,0:T(8,128)(2,1)} async-done(((bf16[2,256,512]{2,1,0:T(8,128)(2,1)}), bf16[2,2048,512]{2,1,0:T(8,128)(2,1)}) %all-gather.11.cloned.1.call-update) | async-done | bytes 4194320 | tf_op jit(solution)/shard_map/all_gather | solution.py:21
  178.6 2.9 fusion.18
  181.5 1.3 collective-permute-start
  182.8 0.0 copy-done.5
  182.8 4.1 collective-permute-done
  187.0 0.2 maximum_convert_fusion
  187.1 64.8 %all-gather.9.cloned.1.call-done = bf16[2,2048,512]{2,1,0:T(8,128)(2,1)} async-done(((bf16[2,256,512]{2,1,0:T(8,128)(2,1)}), bf16[2,2048,512]{2,1,0:T(8,128)(2,1)}) %all-gather.9.cloned.1.call-update) | async-done | bytes 4194320 | tf_op jit(solution)/shard_map/all_gather | solution.py:22
  252.0 74.7 %all-gather.15.cloned.1.call-done = bf16[2,512,2048]{2,1,0:T(8,128)(2,1)} async-done(((bf16[2,512,256]{2,1,0:T(8,128)(2,1)}), bf16[2,512,2048]{2,1,0:T(8,128)(2,1)}) %all-gather.15.cloned.1.call-update) | async-done | bytes 4194320 | tf_op jit(solution)/shard_map/all_gather | solution.py:24
  326.6 6.1 %convolution_convert_fusion.1 = bf16[512,2048]{1,0:T(8,128)(2,1)} fusion(bf16[2,512,2048]{2,1,0:T(8,128)(2,1)} %all-gather.15.cloned.1.call-done, bf16[2,2048,512]{2,1,0:T(8,128)(2,1)} %all-gather.9.cloned.1.call-done, f32[514,512]{1,0:T(8,128)S(1)} %maximum_convert_fusion, f32[512]{0:T(512)S(1)} %bitcast.61, f32[512]{0:T(512)S(1)} %bitcast.62, ...), kind=kOutput, calls=%fused_computation.11 | convolution fusion | flops 2154561536 | bytes 11550720 | tf_op jit(solution)/shard_map/dot_general | solution.py:49
  332.8 0.0 reduce-scatter.3.cloned.1.call-update
  332.8 0.0 all-gather.17.cloned.1.call-start
  332.8 32.2 %reduce-scatter.3.cloned.1.call-done = bf16[512,512]{1,0:T(8,128)(2,1)} async-done(((bf16[512,2048]{1,0:T(8,128)(2,1)}), bf16[512,512]{1,0:T(8,128)(2,1)}) %reduce-scatter.3.cloned.1.call-update) | async-done | bytes 524304 | tf_op jit(solution)/shard_map/reduce_scatter | solution.py:52
  365.1 0.0 copy-done.1
  365.1 2.0 add_convert_fusion.1
  367.0 0.0 all-gather.17.cloned.1.call-update
  367.1 0.0 reduce-scatter.5.cloned.1.call-start
  367.1 22.7 %all-gather.17.cloned.1.call-done = bf16[512,2048]{1,0:T(8,128)(2,1)} async-done(((bf16[512,512]{1,0:T(8,128)(2,1)}), bf16[512,2048]{1,0:T(8,128)(2,1)}) %all-gather.17.cloned.1.call-update) | async-done | bytes 2097168 | tf_op jit(solution)/shard_map/all_gather | solution.py:31
  389.8 2.2 fusion.3
  392.0 0.0 copy-done.3
  392.0 0.0 copy-start.6
  392.0 3.0 fusion.6
  395.1 0.0 copy-done.6
  395.1 1.3 fusion.16
  396.4 1.3 collective-permute-start.1
  397.7 4.2 collective-permute-done.1
  401.9 0.2 maximum_convert_fusion.1
  402.0 6.2 %convolution_convert_fusion = bf16[512,2048]{1,0:T(8,128)(2,1)} fusion(bf16[2,512,2048]{2,1,0:T(8,128)(2,1)} %all-gather.15.cloned.1.call-done, bf16[2,2048,512]{2,1,0:T(8,128)(2,1)} %all-gather.9.cloned.1.call-done, f32[514,512]{1,0:T(8,128)S(1)} %maximum_convert_fusion.1, f32[512]{0:T(512)S(1)} %bitcast.59, f32[512]{0:T(512)S(1)} %bitcast.60, ...), kind=kOutput, calls=%fused_computation.10 | convolution fusion | flops 2154561536 | bytes 11550720 | tf_op jit(solution)/shard_map/dot_general | solution.py:49
  408.2 0.0 reduce-scatter.5.cloned.1.call-update
  408.2 31.3 %reduce-scatter.5.cloned.1.call-done = bf16[512,512]{1,0:T(8,128)(2,1)} async-done(((bf16[512,2048]{1,0:T(8,128)(2,1)}), bf16[512,512]{1,0:T(8,128)(2,1)}) %reduce-scatter.5.cloned.1.call-update) | async-done | bytes 524304 | tf_op jit(solution)/shard_map/reduce_scatter | solution.py:52
  439.6 2.0 add_convert_fusion
  (12 shorter events, 0.1 us)
Async XLA Ops:
  6.5 3.4 copy-start.4
  6.5 25.9 %all-gather.7.cloned.1.call-start = ((), (), s32[]{:S(2)}) async-start(), calls=%async_computation.2 | async-start | bytes 2621440 | tf_op jit(solution)/shard_map/all_gather | solution.py:31
  7.3 97.8 %all-gather.13.cloned.1.call-start = ((), (), s32[]{:S(2)}) async-start(), calls=%async_computation.5 | async-start | bytes 4718592 | tf_op jit(solution)/shard_map/all_gather | solution.py:20
  8.0 170.6 %all-gather.11.cloned.1.call-start = ((), (), s32[]{:S(2)}) async-start(), calls=%async_computation.4 | async-start | bytes 4718592 | tf_op jit(solution)/shard_map/all_gather | solution.py:21
  8.7 243.2 %all-gather.9.cloned.1.call-start = ((), (), s32[]{:S(2)}) async-start(), calls=%async_computation.3 | async-start | bytes 4718592 | tf_op jit(solution)/shard_map/all_gather | solution.py:22
  9.3 317.3 %all-gather.15.cloned.1.call-start = ((), (), s32[]{:S(2)}) async-start(), calls=%async_computation.6 | async-start | bytes 4718592 | tf_op jit(solution)/shard_map/all_gather | solution.py:24
  9.9 355.2 %reduce-scatter.3.cloned.1.call-start = ((), (), s32[]{:S(2)}) async-start(), calls=%async_computation.7 | async-start | bytes 2621440 | tf_op jit(solution)/shard_map/reduce_scatter | solution.py:52
  32.4 72.6 %copy-start.2 = (bf16[512,2048]{1,0:T(8,128)(2,1)S(1)}, bf16[512,2048]{1,0:T(8,128)(2,1)}, u32[]{:S(2)}) copy-start(bf16[512,2048]{1,0:T(8,128)(2,1)} %all-gather.7.cloned.1.call-done) | copy-start | bytes 6291460
  107.9 74.9 %copy-start.5 = (f32[2,3,512]{2,0,1:T(2,128)S(1)}, f32[2,3,512]{2,0,1:T(2,128)}, u32[]{:S(2)}) copy-start(f32[2,3,512]{2,0,1:T(2,128)} %param.12) | copy-start | bytes 36868
  181.5 5.5 %collective-permute-start = (bf16[2,512]{1,0:T(2,128)(2,1)S(1)}, bf16[2,512]{1,0:T(2,128)(2,1)S(1)}, u32[]{:S(2)}, u32[]{:S(2)}) collective-permute-start(bf16[2,512]{1,0:T(2,128)(2,1)S(1)} %slice.113), channel_id=1, source_target_pairs={{0,4},{4,8},{8,12},{12,16},{16,20},{20,24},{24,28},{1,5},{5,9},{9,... | collective-permute-start | bytes 6152 | tf_op jit(solution)/shard_map/ppermute | solution.py:15
  332.8 32.3 %copy-start.1 = (bf16[512,512]{1,0:T(8,128)(2,1)S(1)}, bf16[512,512]{1,0:T(8,128)(2,1)}, u32[]{:S(2)}) copy-start(bf16[512,512]{1,0:T(8,128)(2,1)} %param.7) | copy-start | bytes 1572868
  332.8 57.0 %all-gather.17.cloned.1.call-start = ((), (), s32[]{:S(2)}) async-start(), calls=%async_computation.8 | async-start | bytes 2621440 | tf_op jit(solution)/shard_map/all_gather | solution.py:31
  367.1 72.5 %reduce-scatter.5.cloned.1.call-start = ((), (), s32[]{:S(2)}) async-start(), calls=%async_computation.9 | async-start | bytes 2621440 | tf_op jit(solution)/shard_map/reduce_scatter | solution.py:52
  389.8 2.2 copy-start.3
  392.0 3.1 copy-start.6
  396.4 5.5 %collective-permute-start.1 = (bf16[2,512]{1,0:T(2,128)(2,1)S(1)}, bf16[2,512]{1,0:T(2,128)(2,1)S(1)}, u32[]{:S(2)}, u32[]{:S(2)}) collective-permute-start(bf16[2,512]{1,0:T(2,128)(2,1)S(1)} %slice.121), channel_id=1, source_target_pairs={{0,4},{4,8},{8,12},{12,16},{16,20},{20,24},{24,28},{1,5},{5,9},{9,... | collective-permute-start | bytes 6152 | tf_op jit(solution)/shard_map/ppermute | solution.py:15
  408.2 31.4 %copy-start = (bf16[512,512]{1,0:T(8,128)(2,1)S(1)}, bf16[512,512]{1,0:T(8,128)(2,1)}, u32[]{:S(2)}) copy-start(bf16[512,512]{1,0:T(8,128)(2,1)} %add_convert_fusion.1) | copy-start | bytes 1572868
Sparse Core Ops, SparseCore 0:
  8.9 23.5 all-gather.6
  34.6 70.3 all-gather.12
  107.2 71.2 all-gather.10
  180.6 71.2 all-gather.8
  253.9 72.7 all-gather.14
  332.9 32.1 reduce-scatter.2
  367.2 22.5 all-gather.16
  408.4 31.1 reduce-scatter.4
where the time goes:
time: 450 us; the launch traced here: 448 us
  waiting for transfers between devices  401 us (89%)
  matrix products  22.4 us (5%)
  between operations  13.6 us (3%)
  other arithmetic  8.7 us (2%)
    all_gather x1, waiting for transfers between devices, on_device(): gathered_out = lax.all_gather(w_output, 'sp', axis=2, tiled=True)  74.7 us
    all_gather x1, waiting for transfers between devices, on_device(): lax.all_gather(w_inner, 'sp', axis=1, tiled=True)  70.6 us
    all_gather x1, waiting for transfers between devices, on_device(): lax.all_gather(w_value, 'sp', axis=1, tiled=True)  70.4 us
    all_gather x1, waiting for transfers between devices, on_device(): lax.all_gather(w_outer, 'sp', axis=1, tiled=True)  64.8 us
    reduce_scatter x2, waiting for transfers between devices, on_device(): lax.psum_scatter(terms.astype(jnp.float32).astype(jnp.bfloat16), 'tp', sc...  63.6 us
    all_gather x2, waiting for transfers between devices, on_device(): full_rows = lax.all_gather(stream_now, 'tp', axis=1, tiled=True)  45.1 us
    dot_general x2, matrix products, on_device(): jnp.dot(gated, layer_output, preferred_element_type=jnp.float32)  12.3 us
  transfers between devices with their start and end apart: 10, of which 10 were waited for; matrix products, arithmetic and copies ran while one was open for 2% of the time, Pallas kernels for 0%

commit v1 on v0

v1 whole, which is shorter than its diff:
```python
import functools

import jax
import jax.numpy as jnp
from jax import lax
from jax.experimental import pallas as pl
from jax.experimental.pallas import tpu as pltpu
from jax.sharding import PartitionSpec as P

EPSILON = 1e-06
MESH = pl.DeviceIdType.MESH
F32 = jnp.float32
BF16 = jnp.bfloat16


def kernel(
    dims, stream, gain, w_value, w_inner, w_outer, taps, w_output, out,
    win, wout, held, normed, mix, outer, gated, tsend, s1, r1, r2a, r2b, t3a, t3b,
    r3a, r3b, tail, halo, send_sems, w_recv, swap_recv, local_sems, ag_recv, rs_recv,
):
    L, SP, TP, D, T, kb, nb, cb = dims
    Z = SP // 2
    half = T // 2
    sp, tp = lax.axis_index("sp"), lax.axis_index("tp")
    z, x = sp // 2, lax.rem(sp, 2)
    y, c = tp // 2, lax.rem(tp, 2)
    x_dev = (sp + 1 - 2 * x, tp)
    y_dev = (sp, tp + 2 - 4 * y)
    c_dev = (sp, tp + 1 - 2 * c)
    up_dev = (sp + 2, tp)
    down_dev = (sp - 2, tp)
    has_up, has_down = z < Z - 1, z > 0

    barrier = pltpu.get_barrier_semaphore()
    for dev in (x_dev, y_dev, c_dev):
        pl.semaphore_signal(barrier, inc=1, device_id=dev, device_id_type=MESH)
    for cond, dev in ((has_up, up_dev), (has_down, down_dev)):
        @pl.when(cond)
        def _(dev=dev):
            pl.semaphore_signal(barrier, inc=1, device_id=dev, device_id_type=MESH)
    peers = 3 + has_up.astype(jnp.int32) + has_down.astype(jnp.int32)
    pl.semaphore_wait(barrier, peers)

    sends = []

    def make(src, dst, recv, dev):
        slot = len(sends)
        copy = lambda: pltpu.make_async_remote_copy(
            src_ref=src(), dst_ref=dst(), send_sem=send_sems.at[slot], recv_sem=recv(),
            device_id=dev, device_id_type=MESH)
        return copy

    def send(src, dst, recv, dev):
        copy = make(lambda: src, lambda: dst, lambda: recv, dev)
        sends.append((None, copy))
        copy().start()
        return copy

    def await_recv(ref, sem, dev=x_dev):
        pltpu.make_async_remote_copy(
            src_ref=ref, dst_ref=ref, send_sem=send_sems.at[0], recv_sem=sem,
            device_id=dev, device_id_type=MESH).wait_recv()

    w_in = (w_value, w_inner, w_outer)
    col = lambda q: pl.ds(pl.multiple_of(q * nb, nb), nb)
    krow = lambda s: pl.ds(pl.multiple_of(s * kb, kb), kb)

    def parts(l, s):
        return (win.at[l, :, krow(s), :], wout.at[l, s])

    def swap_parts(l, q, s):
        for i in range(3):
            yield i, w_in[i].at[l, :, col(q)], win.at[l, i, krow(s), :]
        yield 3, w_output.at[l, col(q), :], wout.at[l, s]

    def local_copies(l):
        return [pltpu.make_async_copy(src, dst, local_sems.at[l, i])
                for i, src, dst in swap_parts(l, x, sp)]

    def swap_start(l):
        for i, src, dst in swap_parts(l, 1 - x, sp):
            send(src, dst, swap_recv.at[l, i], x_dev)

    def swap_wait(l):
        for i, src, dst in swap_parts(l, x, x_dev[0]):
            await_recv(dst, swap_recv.at[l, i])

    def relay(l, h, own):
        for sign, neighbour, dev in ((-1, has_up, up_dev), (1, has_down, down_dev)):
            origin = z + sign * h
            cond = jnp.logical_and(neighbour, jnp.logical_and(origin >= 0, origin < Z))
            picks = ((x if own else 1 - x),) if h == 0 else (0, 1)
            group = []
            for p in picks:
                for part in range(2):
                    copy = make(
                        lambda p=p, part=part, origin=origin: parts(l, 2 * origin + p)[part],
                        lambda p=p, part=part, origin=origin: parts(l, 2 * origin + p)[part],
                        lambda p=p, part=part, origin=origin: w_recv.at[l, 2 * origin + p, part],
                        dev)
                    sends.append((cond, copy))
                    group.append((p, part, copy))

            @pl.when(cond)
            def _(group=group, origin=origin, dev=dev):
                for p, part, copy in group:
                    if h > 0:
                        s = 2 * origin + p
                        await_recv(parts(l, s)[part], w_recv.at[l, s, part], dev)
                    copy().start()

    def weights_done(l, part):
        for d in range(1, Z):
            for sign, neighbour in ((-1, has_up), (1, has_down)):
                origin = z + sign * d
                inside = jnp.logical_and(origin >= 0, origin < Z)

                @pl.when(jnp.logical_and(jnp.logical_not(neighbour), inside))
                def _(origin=origin):
                    for p in range(2):
                        s = 2 * origin + p
                        await_recv(parts(l, s)[part], w_recv.at[l, s, part])

    rows_of = {0: pl.ds(0, half), 1: pl.ds(half, half)}

    def gather_start(l):
        for hf, dev in ((1, x_dev), (0, y_dev), (0, x_dev), (1, y_dev)):
            ref = held.at[l, tp, x, rows_of[hf], :]
            send(ref, ref, ag_recv.at[l, tp, x, hf], dev)
        ref = held.at[l, tp, x]
        send(ref, ref, ag_recv.at[l, tp, x, 0], c_dev)

    def gather_rest(l):
        ox, oy = 1 - x, y_dev[1]

        def got(j, xx, hf):
            await_recv(held.at[l, j, xx, rows_of[hf], :], ag_recv.at[l, j, xx, hf])

        got(tp, ox, 1)
        ref = held.at[l, tp, ox, rows_of[1], :]
        send(ref, ref, ag_recv.at[l, tp, ox, 1], y_dev)
        got(oy, x, 0)
        ref = held.at[l, oy, x, rows_of[0], :]
        send(ref, ref, ag_recv.at[l, oy, x, 0], x_dev)
        for j, xx, waits in ((tp, ox, (0,)), (oy, x, (1,)), (oy, ox, (0, 1))):
            for hf in waits:
                got(j, xx, hf)
            ref = held.at[l, j, xx]
            send(ref, ref, ag_recv.at[l, j, xx, 0], c_dev)
        cj, coy = c_dev[1], c_dev[1] + 2 - 4 * y
        for j in (cj, coy):
            for xx in range(2):
                await_recv(held.at[l, j, xx], ag_recv.at[l, j, xx, 0])

    nr = min(128, T)
    per = T // nr

    def normalize(l):
        def body(i, carry):
            xx, r = i // per, lax.rem(i, per)
            rows = pl.ds(pl.multiple_of(r * nr, nr), nr)
            blocks = [held[l, j, xx, rows, :].astype(F32) for j in range(TP)]
            total = sum(jnp.sum(b * b, axis=-1, keepdims=True) for b in blocks)
            scale = lax.rsqrt(total * (1.0 / D) + EPSILON)
            to = pl.ds(pl.multiple_of(i * nr, nr), nr)
            for j in range(TP):
                g = gain[l:l + 1, j * cb:(j + 1) * cb]
                normed[to, j * cb:(j + 1) * cb] = (blocks[j] * scale * g).astype(BF16)
            return carry
        lax.fori_loop(0, 2 * per, body, 0)

    mb = min(256, T)
    mper = T // mb

    def project(l):
        def body(i, carry):
            rows = pl.ds(pl.multiple_of(i * mb, mb), mb)
            n = normed[rows, :]
            v = jnp.dot(n, win[l, 0], preferred_element_type=F32)
            g = jnp.dot(n, win[l, 1], preferred_element_type=F32)
            mix[pl.ds(pl.multiple_of(16 + i * mb, 16), mb), :] = (g * v).astype(BF16).astype(F32)
            outer[rows, :] = jnp.dot(n, win[l, 2], preferred_element_type=F32)
            return carry
        lax.fori_loop(0, 2 * mper, body, 0)
        tail[l] = mix[2 * T:2 * T + 16, :].astype(BF16)
        copy = make(lambda: tail.at[l], lambda: halo.at[l], lambda: rs_recv.at[l, 0], up_dev)
        sends.append((has_up, copy))

        @pl.when(has_up)
        def _():
            copy().start()

    def w_block(l, j):
        per_tp = SP // TP
        return jnp.concatenate([wout[l, j * per_tp + q] for q in range(per_tp)], axis=1)

    def convolve(l):
        mix[0:16, :] = jnp.zeros((16, nb), F32)

        @pl.when(has_down)
        def _():
            await_recv(halo.at[l], rs_recv.at[l, 0])
            mix[0:16, :] = halo[l].astype(F32)

        tap = taps[l, :, col(x)]

        def body(i, carry):
            m = mix[pl.ds(pl.multiple_of(8 + i * mb, 8), mb + 8), :]
            conv = tap[0:1] * m[6:6 + mb] + tap[1:2] * m[7:7 + mb] + tap[2:3] * m[8:8 + mb]
            rows = pl.ds(pl.multiple_of(i * mb, mb), mb)
            gated[rows, :] = (outer[rows, :] * conv).astype(BF16)
            return carry
        lax.fori_loop(0, 2 * mper, body, 0)

    def outputs(l, target, core, finish):
        for yj in range(2):
            j = 2 * yj + core
            w = w_block(l, j)

            def body(i, carry):
                xx, r = i // mper, lax.rem(i, mper)
                g = gated[pl.ds(pl.multiple_of(i * mb, mb), mb), :]
                t = jnp.dot(g, w, preferred_element_type=F32).astype(BF16)
                rows = pl.ds(pl.multiple_of(r * mb, mb), mb)
                if finish:
                    t = (t.astype(F32) + r1[l, yj, xx, rows, :].astype(F32)).astype(BF16)
                target[l, yj, xx, rows, :] = t
                return carry
            if finish:
                await_recv(r1.at[l, yj], rs_recv.at[l, 1 + yj])
            lax.fori_loop(0, 2 * mper, body, 0)
            if not finish:
                send(tsend.at[l, yj], r1.at[l, yj], rs_recv.at[l, 1 + yj], c_dev)

    def f(ref):
        return ref.astype(F32)

    def reduce(l, store):
        A, B = rows_of[0], rows_of[1]
        send(s1.at[l, :, 1 - x, A, :], r2a.at[l], rs_recv.at[l, 3], x_dev)
        send(s1.at[l, 1 - y, :, B, :], r2b.at[l], rs_recv.at[l, 4], y_dev)
        await_recv(r2a.at[l], rs_recv.at[l, 3])
        t3a[l] = (f(s1[l, 1 - y, x, A, :]) + f(r2a[l, 1 - y])).astype(BF16)
        send(t3a.at[l], r3a.at[l], rs_recv.at[l, 5], y_dev)
        await_recv(r2b.at[l], rs_recv.at[l, 4])
        t3b[l] = (f(s1[l, y, 1 - x, B, :]) + f(r2b[l, 1 - x])).astype(BF16)
        send(t3b.at[l], r3b.at[l], rs_recv.at[l, 6], x_dev)
        await_recv(r3a.at[l], rs_recv.at[l, 5])
        branch = f(s1[l, y, x, A, :]) + f(r2a[l, y]) + f(r3a[l])
        store(A, (f(held[l, tp, x, A, :]) + branch).astype(BF16))
        await_recv(r3b.at[l], rs_recv.at[l, 6])
        branch = f(s1[l, y, x, B, :]) + f(r2b[l, x]) + f(r3b[l])
        store(B, (f(held[l, tp, x, B, :]) + branch).astype(BF16))

    copies = [local_copies(l) for l in range(L)]
    for group in copies:
        for copy in group:
            copy.start()
    swap_start(0)
    for copy in copies[0]:
        copy.wait()
    relay(0, 0, True)
    held[0, tp, x] = stream[...]
    gather_start(0)
    swap_wait(0)
    relay(0, 0, False)
    gather_rest(0)
    for l in range(1, L):
        swap_start(l)
    normalize(0)
    for h in range(1, Z - 1):
        relay(0, h, True)
    for l in range(L):
        if l + 1 < L:
            for copy in copies[l + 1]:
                copy.wait()
            swap_wait(l + 1)
            relay(l + 1, 0, True)
            relay(l + 1, 0, False)
        weights_done(l, 0)
        project(l)
        convolve(l)
        weights_done(l, 1)
        outputs(l, tsend, 1 - c, False)
        outputs(l, s1, c, True)
        if l + 1 < L:
            def store(rows, value, l=l):
                held[l + 1, tp, x, rows, :] = value
            reduce(l, store)
            gather_start(l + 1)
            if Z > 2:
                relay(l + 1, 1, True)
            gather_rest(l + 1)
            normalize(l + 1)
            for h in range(2, Z - 1):
                relay(l + 1, h, True)
        else:
            def store(rows, value):
                out[rows, :] = value
            reduce(l, store)

    for cond, copy in sends:
        if cond is None:
            copy().wait_send()
        else:
            @pl.when(cond)
            def _(copy=copy):
                copy().wait_send()


def on_device(SP, TP, stream, norm_gain, w_value, w_inner, w_outer, conv_taps, w_output):
    L, kb, cb = w_value.shape
    T, D = stream.shape[0], norm_gain.shape[1]
    nb, Z = cb // 2, SP // 2
    dims = (L, SP, TP, D, T, kb, nb, cb)
    vmem = pl.BlockSpec(memory_space=pltpu.VMEM)
    hbm = pl.BlockSpec(memory_space=pl.ANY)
    half = T // 2
    n_sends = L * (4 + 4 * (1 + 2 * max(Z - 2, 0)) * 2 + 16 + 8)
    return pl.pallas_call(
        functools.partial(kernel, dims),
        out_shape=jax.ShapeDtypeStruct((T, cb), BF16),
        in_specs=[vmem, vmem, hbm, hbm, hbm, vmem, hbm],
        out_specs=vmem,
        scratch_shapes=[
            pltpu.VMEM((L, 3, D, nb), BF16),
            pltpu.VMEM((L, SP, nb, kb), BF16),
            pltpu.VMEM((L, TP, 2, T, cb), BF16),
            pltpu.VMEM((2 * T, D), BF16),
            pltpu.VMEM((2 * T + 16, nb), F32),
            pltpu.VMEM((2 * T, nb), F32),
            pltpu.VMEM((2 * T, nb), BF16),
            pltpu.VMEM((L, 2, 2, T, cb), BF16),
            pltpu.VMEM((L, 2, 2, T, cb), BF16),
            pltpu.VMEM((L, 2, 2, T, cb), BF16),
            pltpu.VMEM((L, 2, half, cb), BF16),
            pltpu.VMEM((L, 2, half, cb), BF16),
            pltpu.VMEM((L, half, cb), BF16),
            pltpu.VMEM((L, half, cb), BF16),
            pltpu.VMEM((L, half, cb), BF16),
            pltpu.VMEM((L, half, cb), BF16),
            pltpu.VMEM((L, 16, nb), BF16),
            pltpu.VMEM((L, 16, nb), BF16),
            pltpu.SemaphoreType.DMA((n_sends,)),
            pltpu.SemaphoreType.DMA((L, SP, 2)),
            pltpu.SemaphoreType.DMA((L, 4)),
            pltpu.SemaphoreType.DMA((L, 4)),
            pltpu.SemaphoreType.DMA((L, TP, 2, 2)),
            pltpu.SemaphoreType.DMA((L, 7)),
        ],
        compiler_params=pltpu.CompilerParams(
            collective_id=0, has_side_effects=True, vmem_limit_bytes=60 * 1024 * 1024
        ),
    )(stream, norm_gain, w_value, w_inner, w_outer, conv_taps, w_output)


def solution(mesh):
    SP, TP = mesh.shape["sp"], mesh.shape["tp"]
    in_specs = (
        P("sp", "tp"),
        P(),
        P(None, "sp", "tp"),
        P(None, "sp", "tp"),
        P(None, "sp", "tp"),
        P(None, None, "tp"),
        P(None, "tp", "sp"),
    )
    return jax.shard_map(
        functools.partial(on_device, SP, TP),
        mesh=mesh, in_specs=in_specs, out_specs=P("sp", "tp"), check_vma=False,
    )
```

time: 450 us -> 194 us (0.43)
  waiting for transfers between devices: 401 us -> 0 us
  Pallas kernels: 0 us -> 189 us
  matrix products: 22.4 us -> 0 us
  between operations: 13.6 us -> 0.01 us
  other arithmetic: 8.7 us -> 0 us
    all_gather x6 -> x0, waiting for transfers between devices: 326 us -> none  [the longest x1 74.7 us: on_device(): gathered_out = lax.all_gather(w_output, 'sp', axis=2, tiled=True)]
    pallas_call x0 -> x1, Pallas kernels: none -> 189 us  [on_device(): pl.pallas_call(functools.partial(kernel, dims), out_shape=jax.ShapeDtypeS...]
    reduce_scatter x2 -> x0, waiting for transfers between devices: 63.6 us -> none  [on_device(): lax.psum_scatter(terms.astype(jnp.float32).astype(jnp.bfloat16), 'tp', sc...]
    dot_general x6 -> x0, matrix products: 22.4 us -> none  [the longest x2 12.3 us: on_device(): jnp.dot(gated, layer_output, preferred_element_type=jnp.float32)]
    ppermute x2 -> x0, waiting for transfers between devices: 8.33 us -> none  [passed_along(): return lax.ppermute(block, axis, route)]
  transfers between devices with their start and end apart: 10 -> 0, of which waited for: 10 -> 0; matrix products, arithmetic and copies ran while one was open for 2% -> 0% of each run, Pallas kernels for 0% -> 0%
where the time goes in v1:
time: 194 us; the launch traced here: 192 us
  Pallas kernels  189 us (97%)
  local copies, waits for them, and re-layouts  3.18 us (2%)
    pallas_call x1, Pallas kernels, on_device(): pl.pallas_call(functools.partial(kernel, dims), out_shape=jax.ShapeDtypeS...  189 us

profile of v1, /device:TPU:26, one launch (start us, length us, event | category | flops | bytes accessed | tf_op | source)
XLA Modules:
  0.0 191.8 jit_solution(550084820293850425)
XLA Ops:
  0.0 1.3 copy.8.taps
  1.3 188.6 %shard_map.73 = bf16[512,512]{1,0:T(8,128)(2,1)} custom-call(bf16[512,512]{1,0:T(8,128)(2,1)} %stream.1, f32[2,2048]{1,0:T(2,128)} %gain.1, bf16[2,256,512]{2,1,0:T(8,128)(2,1)} %w_value.1, bf16[2,256,512]{2,1,0:T(8,128)(2,1)} %w_inner.1, bf16[2,256,512]{2,1,0:T(8,128)(2,1)} %w_outer.1, f32[2,3,512]{2,1,0:T(4,128)} %copy.8.taps, bf16[2,512,256]{2,1,0:T(8,128)(2,1)} %w_output.1), custom_call_target="tpu_custom_call" | custom-call | tf_op jit(solution)/shard_map/pallas_call | solution.py:320
  189.9 1.9 copy.10

commit v2 on v1

--- a/solution.py
+++ b/solution.py
@@ -85,27 +85,32 @@
         for i, src, dst in swap_parts(l, x, x_dev[0]):
             await_recv(dst, swap_recv.at[l, i])
 
-    def relay(l, h, own):
+    middle = jnp.logical_and(has_up, has_down)
+    ends = jnp.logical_not(middle)
+    IN, OUT = 0, 1
+
+    def relay(l, part, h, picks=None, only=None):
         for sign, neighbour, dev in ((-1, has_up, up_dev), (1, has_down, down_dev)):
             origin = z + sign * h
             cond = jnp.logical_and(neighbour, jnp.logical_and(origin >= 0, origin < Z))
-            picks = ((x if own else 1 - x),) if h == 0 else (0, 1)
+            if only is not None:
+                cond = jnp.logical_and(cond, only)
             group = []
-            for p in picks:
-                for part in range(2):
-                    copy = make(
-                        lambda p=p, part=part, origin=origin: parts(l, 2 * origin + p)[part],
-                        lambda p=p, part=part, origin=origin: parts(l, 2 * origin + p)[part],
-                        lambda p=p, part=part, origin=origin: w_recv.at[l, 2 * origin + p, part],
-                        dev)
-                    sends.append((cond, copy))
-                    group.append((p, part, copy))
+            for p in (picks or (x, 1 - x)):
+                s = 2 * origin + p
+
+                def copy(s=s, dev=dev, slot=len(sends)):
+                    ref = parts(l, s)[part]
+                    return pltpu.make_async_remote_copy(
+                        src_ref=ref, dst_ref=ref, send_sem=send_sems.at[slot],
+                        recv_sem=w_recv.at[l, s, part], device_id=dev, device_id_type=MESH)
+                sends.append((cond, copy))
+                group.append((s, copy))
 
             @pl.when(cond)
-            def _(group=group, origin=origin, dev=dev):
-                for p, part, copy in group:
+            def _(group=group, dev=dev):
+                for s, copy in group:
                     if h > 0:
-                        s = 2 * origin + p
                         await_recv(parts(l, s)[part], w_recv.at[l, s, part], dev)
                     copy().start()
 
@@ -259,41 +264,53 @@
     swap_start(0)
     for copy in copies[0]:
         copy.wait()
-    relay(0, 0, True)
+    relay(0, IN, 0, (x,))
     held[0, tp, x] = stream[...]
     gather_start(0)
     swap_wait(0)
-    relay(0, 0, False)
+    relay(0, IN, 0, (1 - x,))
+    relay(0, OUT, 0, only=ends)
+    if Z > 2:
+        relay(0, IN, 1)
     gather_rest(0)
     for l in range(1, L):
         swap_start(l)
+    for h in range(2, Z - 1):
+        relay(0, IN, h)
+    relay(0, OUT, 0, only=middle)
     normalize(0)
-    for h in range(1, Z - 1):
-        relay(0, h, True)
+    for l in range(1, L):
+        for copy in copies[l]:
+            copy.wait()
+        swap_wait(l)
+        relay(l, IN, 0, only=ends)
+        relay(l, OUT, 0, only=ends)
     for l in range(L):
+        weights_done(l, IN)
+        project(l)
         if l + 1 < L:
-            for copy in copies[l + 1]:
-                copy.wait()
-            swap_wait(l + 1)
-            relay(l + 1, 0, True)
-            relay(l + 1, 0, False)
-        weights_done(l, 0)
-        project(l)
+            for h in range(1, Z - 1):
+                relay(l, OUT, h)
+            relay(l + 1, IN, 0, only=middle)
         convolve(l)
-        weights_done(l, 1)
+        weights_done(l, OUT)
         outputs(l, tsend, 1 - c, False)
         outputs(l, s1, c, True)
         if l + 1 < L:
             def store(rows, value, l=l):
                 held[l + 1, tp, x, rows, :] = value
+            if Z > 2:
+                relay(l + 1, IN, 1)
             reduce(l, store)
             gather_start(l + 1)
-            if Z > 2:
-                relay(l + 1, 1, True)
+            for h in range(2, Z - 1):
+                relay(l + 1, IN, h)
             gather_rest(l + 1)
+            relay(l + 1, OUT, 0, only=middle)
             normalize(l + 1)
-            for h in range(2, Z - 1):
-                relay(l + 1, h, True)
+            if l + 2 == L:
+                for h in range(1, Z - 1):
+                    relay(l + 1, OUT, h)
         else:
             def store(rows, value):
                 out[rows, :] = value
@@ -316,7 +333,7 @@
     vmem = pl.BlockSpec(memory_space=pltpu.VMEM)
     hbm = pl.BlockSpec(memory_space=pl.ANY)
     half = T // 2
-    n_sends = L * (4 + 4 * (1 + 2 * max(Z - 2, 0)) * 2 + 16 + 8)
+    n_sends = L * (4 + 8 * max(Z - 1, 1) + 8 + 9 + 8)
     return pl.pallas_call(
         functools.partial(kernel, dims),
         out_shape=jax.ShapeDtypeStruct((T, cb), BF16),

time: 194 us -> 175 us (0.902)
  Pallas kernels: 189 us -> 170 us
    pallas_call x1, Pallas kernels: 189 us -> 170 us  [on_device(): pl.pallas_call(functools.partial(kernel, dims), out_shape=jax.ShapeDtypeS...]
where the time goes in v2:
time: 175 us; the launch traced here: 173 us
  Pallas kernels  170 us (97%)
  local copies, waits for them, and re-layouts  3.18 us (2%)
    pallas_call x1, Pallas kernels, on_device(): pl.pallas_call(functools.partial(kernel, dims), out_shape=jax.ShapeDtypeS...  170 us

profile of v2, /device:TPU:26, one launch (start us, length us, event | category | flops | bytes accessed | tf_op | source)
XLA Modules:
  0.0 173.1 jit_solution(9991744499063738932)
XLA Ops:
  0.0 1.3 copy.8.taps
  1.3 169.9 %shard_map.73 = bf16[512,512]{1,0:T(8,128)(2,1)} custom-call(bf16[512,512]{1,0:T(8,128)(2,1)} %stream.1, f32[2,2048]{1,0:T(2,128)} %gain.1, bf16[2,256,512]{2,1,0:T(8,128)(2,1)} %w_value.1, bf16[2,256,512]{2,1,0:T(8,128)(2,1)} %w_inner.1, bf16[2,256,512]{2,1,0:T(8,128)(2,1)} %w_outer.1, f32[2,3,512]{2,1,0:T(4,128)} %copy.8.taps, bf16[2,512,256]{2,1,0:T(8,128)(2,1)} %w_output.1), custom_call_target="tpu_custom_call" | custom-call | tf_op jit(solution)/shard_map/pallas_call | solution.py:337
  171.2 1.9 %copy.10 = bf16[512,512]{1,0:T(8,128)(2,1)} copy(bf16[512,512]{1,0:T(8,128)(2,1)} %shard_map.73) | data formatting | bytes 1048576

commit v3 on v2

--- a/solution.py
+++ b/solution.py
@@ -31,16 +31,7 @@
     down_dev = (sp - 2, tp)
     has_up, has_down = z < Z - 1, z > 0
 
-    barrier = pltpu.get_barrier_semaphore()
-    for dev in (x_dev, y_dev, c_dev):
-        pl.semaphore_signal(barrier, inc=1, device_id=dev, device_id_type=MESH)
-    for cond, dev in ((has_up, up_dev), (has_down, down_dev)):
-        @pl.when(cond)
-        def _(dev=dev):
-            pl.semaphore_signal(barrier, inc=1, device_id=dev, device_id_type=MESH)
-    peers = 3 + has_up.astype(jnp.int32) + has_down.astype(jnp.int32)
-    pl.semaphore_wait(barrier, peers)
-
+    first = (2 * z >= Z).astype(jnp.int32)
     sends = []
 
     def make(src, dst, recv, dev):
@@ -81,22 +72,22 @@
         for i, src, dst in swap_parts(l, 1 - x, sp):
             send(src, dst, swap_recv.at[l, i], x_dev)
 
-    def swap_wait(l):
+    def swap_wait(l, part):
         for i, src, dst in swap_parts(l, x, x_dev[0]):
-            await_recv(dst, swap_recv.at[l, i])
+            if (i == 3) == (part == OUT):
+                await_recv(dst, swap_recv.at[l, i])
 
     middle = jnp.logical_and(has_up, has_down)
     ends = jnp.logical_not(middle)
     IN, OUT = 0, 1
 
     def relay(l, part, h, picks=None, only=None):
-        for sign, neighbour, dev in ((-1, has_up, up_dev), (1, has_down, down_dev)):
-            origin = z + sign * h
-            cond = jnp.logical_and(neighbour, jnp.logical_and(origin >= 0, origin < Z))
-            if only is not None:
-                cond = jnp.logical_and(cond, only)
-            group = []
-            for p in (picks or (x, 1 - x)):
+        for p in (picks or (x, 1 - x)):
+            for sign, neighbour, dev in ((-1, has_up, up_dev), (1, has_down, down_dev)):
+                origin = z + sign * h
+                cond = jnp.logical_and(neighbour, jnp.logical_and(origin >= 0, origin < Z))
+                if only is not None:
+                    cond = jnp.logical_and(cond, only)
                 s = 2 * origin + p
 
                 def copy(s=s, dev=dev, slot=len(sends)):
@@ -105,20 +96,21 @@
                         src_ref=ref, dst_ref=ref, send_sem=send_sems.at[slot],
                         recv_sem=w_recv.at[l, s, part], device_id=dev, device_id_type=MESH)
                 sends.append((cond, copy))
-                group.append((s, copy))
-
-            @pl.when(cond)
-            def _(group=group, dev=dev):
-                for s, copy in group:
+
+                @pl.when(cond)
+                def _(s=s, copy=copy, dev=dev):
                     if h > 0:
                         await_recv(parts(l, s)[part], w_recv.at[l, s, part], dev)
                     copy().start()
 
-    def weights_done(l, part):
+    def weights_done(l, part, near=None):
         for d in range(1, Z):
             for sign, neighbour in ((-1, has_up), (1, has_down)):
                 origin = z + sign * d
                 inside = jnp.logical_and(origin >= 0, origin < Z)
+                if near is not None:
+                    same = (2 * origin >= Z) == (first == 1)
+                    inside = jnp.logical_and(inside, same if near else jnp.logical_not(same))
 
                 @pl.when(jnp.logical_and(jnp.logical_not(neighbour), inside))
                 def _(origin=origin):
@@ -217,43 +209,57 @@
             return carry
         lax.fori_loop(0, 2 * mper, body, 0)
 
-    def outputs(l, target, core, finish):
-        for yj in range(2):
-            j = 2 * yj + core
-            w = w_block(l, j)
-
-            def body(i, carry):
-                xx, r = i // mper, lax.rem(i, mper)
-                g = gated[pl.ds(pl.multiple_of(i * mb, mb), mb), :]
-                t = jnp.dot(g, w, preferred_element_type=F32).astype(BF16)
-                rows = pl.ds(pl.multiple_of(r * mb, mb), mb)
-                if finish:
-                    t = (t.astype(F32) + r1[l, yj, xx, rows, :].astype(F32)).astype(BF16)
-                target[l, yj, xx, rows, :] = t
-                return carry
+    def outputs(l, yj, target, core, finish):
+        w = w_block(l, 2 * yj + core)
+
+        def body(i, carry):
+            xx, r = i // mper, lax.rem(i, mper)
+            g = gated[pl.ds(pl.multiple_of(i * mb, mb), mb), :]
+            t = jnp.dot(g, w, preferred_element_type=F32).astype(BF16)
+            rows = pl.ds(pl.multiple_of(r * mb, mb), mb)
             if finish:
-                await_recv(r1.at[l, yj], rs_recv.at[l, 1 + yj])
-            lax.fori_loop(0, 2 * mper, body, 0)
-            if not finish:
-                send(tsend.at[l, yj], r1.at[l, yj], rs_recv.at[l, 1 + yj], c_dev)
+                t = (t.astype(F32) + r1[l, yj, xx, rows, :].astype(F32)).astype(BF16)
+            target[l, yj, xx, rows, :] = t
+            return carry
+        if finish:
+            await_recv(r1.at[l, yj], rs_recv.at[l, 1 + yj])
+        lax.fori_loop(0, 2 * mper, body, 0)
+        if not finish:
+            send(tsend.at[l, yj], r1.at[l, yj], rs_recv.at[l, 1 + yj], c_dev)
+
+    def output_group(l, yj):
+        A, B = rows_of[0], rows_of[1]
+        outputs(l, yj, tsend, 1 - c, False)
+        outputs(l, yj, s1, c, True)
+        send(s1.at[l, yj, 1 - x, A, :], r2a.at[l, yj], rs_recv.at[l, 3 + yj], x_dev)
+        other = yj != y
+        for xj in (1 - x, x):
+            copy = make(
+                lambda xj=xj: s1.at[l, yj, xj, B, :], lambda xj=xj: r2b.at[l, xj],
+                lambda xj=xj: rs_recv.at[l, 5 + xj], y_dev)
+            sends.append((other, copy))
+
+            @pl.when(other)
+            def _(copy=copy):
+                copy().start()
 
     def f(ref):
         return ref.astype(F32)
 
     def reduce(l, store):
         A, B = rows_of[0], rows_of[1]
-        send(s1.at[l, :, 1 - x, A, :], r2a.at[l], rs_recv.at[l, 3], x_dev)
-        send(s1.at[l, 1 - y, :, B, :], r2b.at[l], rs_recv.at[l, 4], y_dev)
-        await_recv(r2a.at[l], rs_recv.at[l, 3])
+        await_recv(r2a.at[l, 1 - y], rs_recv.at[l, 4 - y])
         t3a[l] = (f(s1[l, 1 - y, x, A, :]) + f(r2a[l, 1 - y])).astype(BF16)
-        send(t3a.at[l], r3a.at[l], rs_recv.at[l, 5], y_dev)
-        await_recv(r2b.at[l], rs_recv.at[l, 4])
+        send(t3a.at[l], r3a.at[l], rs_recv.at[l, 7], y_dev)
+        await_recv(r2b.at[l, 1 - x], rs_recv.at[l, 6 - x])
         t3b[l] = (f(s1[l, y, 1 - x, B, :]) + f(r2b[l, 1 - x])).astype(BF16)
-        send(t3b.at[l], r3b.at[l], rs_recv.at[l, 6], x_dev)
-        await_recv(r3a.at[l], rs_recv.at[l, 5])
+        send(t3b.at[l], r3b.at[l], rs_recv.at[l, 8], x_dev)
+        await_recv(r2a.at[l, y], rs_recv.at[l, 3 + y])
+        await_recv(r3a.at[l], rs_recv.at[l, 7])
         branch = f(s1[l, y, x, A, :]) + f(r2a[l, y]) + f(r3a[l])
         store(A, (f(held[l, tp, x, A, :]) + branch).astype(BF16))
-        await_recv(r3b.at[l], rs_recv.at[l, 6])
+        await_recv(r2b.at[l, x], rs_recv.at[l, 5 + x])
+        await_recv(r3b.at[l], rs_recv.at[l, 8])
         branch = f(s1[l, y, x, B, :]) + f(r2b[l, x]) + f(r3b[l])
         store(B, (f(held[l, tp, x, B, :]) + branch).astype(BF16))
 
@@ -261,15 +267,29 @@
     for group in copies:
         for copy in group:
             copy.start()
+    held[0, tp, x] = stream[...]
+
+    barrier = pltpu.get_barrier_semaphore()
+    for dev in (x_dev, y_dev, c_dev):
+        pl.semaphore_signal(barrier, inc=1, device_id=dev, device_id_type=MESH)
+    for cond, dev in ((has_up, up_dev), (has_down, down_dev)):
+        @pl.when(cond)
+        def _(dev=dev):
+            pl.semaphore_signal(barrier, inc=1, device_id=dev, device_id_type=MESH)
+    peers = 3 + has_up.astype(jnp.int32) + has_down.astype(jnp.int32)
+    pl.semaphore_wait(barrier, peers)
+
     swap_start(0)
-    for copy in copies[0]:
+    for copy in copies[0][:3]:
         copy.wait()
     relay(0, IN, 0, (x,))
-    held[0, tp, x] = stream[...]
+    copies[0][3].wait()
+    relay(0, OUT, 0, (x,))
     gather_start(0)
-    swap_wait(0)
+    swap_wait(0, IN)
     relay(0, IN, 0, (1 - x,))
-    relay(0, OUT, 0, only=ends)
+    swap_wait(0, OUT)
+    relay(0, OUT, 0, (1 - x,), only=ends)
     if Z > 2:
         relay(0, IN, 1)
     gather_rest(0)
@@ -277,12 +297,13 @@
         swap_start(l)
     for h in range(2, Z - 1):
         relay(0, IN, h)
-    relay(0, OUT, 0, only=middle)
+    relay(0, OUT, 0, (1 - x,), only=middle)
     normalize(0)
     for l in range(1, L):
         for copy in copies[l]:
             copy.wait()
-        swap_wait(l)
+        swap_wait(l, IN)
+        swap_wait(l, OUT)
         relay(l, IN, 0, only=ends)
         relay(l, OUT, 0, only=ends)
     for l in range(L):
@@ -293,9 +314,10 @@
                 relay(l, OUT, h)
             relay(l + 1, IN, 0, only=middle)
         convolve(l)
-        weights_done(l, OUT)
-        outputs(l, tsend, 1 - c, False)
-        outputs(l, s1, c, True)
+        weights_done(l, OUT, True)
+        output_group(l, first)
+        weights_done(l, OUT, False)
+        output_group(l, 1 - first)
         if l + 1 < L:
             def store(rows, value, l=l):
                 held[l + 1, tp, x, rows, :] = value
@@ -333,7 +355,7 @@
     vmem = pl.BlockSpec(memory_space=pltpu.VMEM)
     hbm = pl.BlockSpec(memory_space=pl.ANY)
     half = T // 2
-    n_sends = L * (4 + 8 * max(Z - 1, 1) + 8 + 9 + 8)
+    n_sends = L * (4 + 8 * max(Z - 1, 1) + 8 + 10 + 13)
     return pl.pallas_call(
         functools.partial(kernel, dims),
         out_shape=jax.ShapeDtypeStruct((T, cb), BF16),
@@ -363,7 +385,7 @@
             pltpu.SemaphoreType.DMA((L, 4)),
             pltpu.SemaphoreType.DMA((L, 4)),
             pltpu.SemaphoreType.DMA((L, TP, 2, 2)),
-            pltpu.SemaphoreType.DMA((L, 7)),
+            pltpu.SemaphoreType.DMA((L, 9)),
         ],
         compiler_params=pltpu.CompilerParams(
             collective_id=0, has_side_effects=True, vmem_limit_bytes=60 * 1024 * 1024

time: 175 us -> 173 us (0.989)
  no operation moved by 1% of the time
where the time goes in v3:
time: 173 us; the launch traced here: 172 us
  Pallas kernels  169 us (98%)
  local copies, waits for them, and re-layouts  3.18 us (2%)
    pallas_call x1, Pallas kernels, on_device(): pl.pallas_call(functools.partial(kernel, dims), out_shape=jax.ShapeDtypeS...  169 us

profile of v3, /device:TPU:26, one launch (start us, length us, event | category | flops | bytes accessed | tf_op | source)
XLA Modules:
  0.0 172.3 jit_solution(5707658765113678421)
XLA Ops:
  0.0 1.3 copy.8.taps
  1.3 169.2 %shard_map.73 = bf16[512,512]{1,0:T(8,128)(2,1)} custom-call(bf16[512,512]{1,0:T(8,128)(2,1)} %stream.1, f32[2,2048]{1,0:T(2,128)} %gain.1, bf16[2,256,512]{2,1,0:T(8,128)(2,1)} %w_value.1, bf16[2,256,512]{2,1,0:T(8,128)(2,1)} %w_inner.1, bf16[2,256,512]{2,1,0:T(8,128)(2,1)} %w_outer.1, f32[2,3,512]{2,1,0:T(4,128)} %copy.8.taps, bf16[2,512,256]{2,1,0:T(8,128)(2,1)} %w_output.1), custom_call_target="tpu_custom_call" | custom-call | tf_op jit(solution)/shard_map/pallas_call | solution.py:359
  170.5 1.9 %copy.10 = bf16[512,512]{1,0:T(8,128)(2,1)} copy(bf16[512,512]{1,0:T(8,128)(2,1)} %shard_map.73) | data formatting | bytes 1048576

commit v4 on v3

--- a/solution.py
+++ b/solution.py
@@ -166,19 +166,20 @@
             return carry
         lax.fori_loop(0, 2 * per, body, 0)
 
+    pb = T
     mb = min(256, T)
     mper = T // mb
 
     def project(l):
         def body(i, carry):
-            rows = pl.ds(pl.multiple_of(i * mb, mb), mb)
+            rows = pl.ds(pl.multiple_of(i * pb, pb), pb)
             n = normed[rows, :]
             v = jnp.dot(n, win[l, 0], preferred_element_type=F32)
             g = jnp.dot(n, win[l, 1], preferred_element_type=F32)
-            mix[pl.ds(pl.multiple_of(16 + i * mb, 16), mb), :] = (g * v).astype(BF16).astype(F32)
+            mix[pl.ds(pl.multiple_of(16 + i * pb, 16), pb), :] = (g * v).astype(BF16).astype(F32)
             outer[rows, :] = jnp.dot(n, win[l, 2], preferred_element_type=F32)
             return carry
-        lax.fori_loop(0, 2 * mper, body, 0)
+        lax.fori_loop(0, 2, body, 0)
         tail[l] = mix[2 * T:2 * T + 16, :].astype(BF16)
         copy = make(lambda: tail.at[l], lambda: halo.at[l], lambda: rs_recv.at[l, 0], up_dev)
         sends.append((has_up, copy))
@@ -213,17 +214,15 @@
         w = w_block(l, 2 * yj + core)
 
         def body(i, carry):
-            xx, r = i // mper, lax.rem(i, mper)
-            g = gated[pl.ds(pl.multiple_of(i * mb, mb), mb), :]
+            g = gated[pl.ds(pl.multiple_of(i * pb, pb), pb), :]
             t = jnp.dot(g, w, preferred_element_type=F32).astype(BF16)
-            rows = pl.ds(pl.multiple_of(r * mb, mb), mb)
             if finish:
-                t = (t.astype(F32) + r1[l, yj, xx, rows, :].astype(F32)).astype(BF16)
-            target[l, yj, xx, rows, :] = t
+                t = (t.astype(F32) + r1[l, yj, i].astype(F32)).astype(BF16)
+            target[l, yj, i] = t
             return carry
         if finish:
             await_recv(r1.at[l, yj], rs_recv.at[l, 1 + yj])
-        lax.fori_loop(0, 2 * mper, body, 0)
+        lax.fori_loop(0, 2, body, 0)
         if not finish:
             send(tsend.at[l, yj], r1.at[l, yj], rs_recv.at[l, 1 + yj], c_dev)
 
@@ -309,9 +308,9 @@
     for l in range(L):
         weights_done(l, IN)
         project(l)
+        for h in range(1, Z - 1):
+            relay(l, OUT, h)
         if l + 1 < L:
-            for h in range(1, Z - 1):
-                relay(l, OUT, h)
             relay(l + 1, IN, 0, only=middle)
         convolve(l)
         weights_done(l, OUT, True)
@@ -330,9 +329,6 @@
             gather_rest(l + 1)
             relay(l + 1, OUT, 0, only=middle)
             normalize(l + 1)
-            if l + 2 == L:
-                for h in range(1, Z - 1):
-                    relay(l + 1, OUT, h)
         else:
             def store(rows, value):
                 out[rows, :] = value

time: 173 us -> 168 us (0.971)
  Pallas kernels: 169 us -> 163 us
    pallas_call x1, Pallas kernels: 169 us -> 163 us  [on_device(): pl.pallas_call(functools.partial(kernel, dims), out_shape=jax.ShapeDtypeS...]
where the time goes in v4:
time: 168 us; the launch traced here: 166 us
  Pallas kernels  163 us (97%)
  local copies, waits for them, and re-layouts  3.18 us (2%)
    pallas_call x1, Pallas kernels, on_device(): pl.pallas_call(functools.partial(kernel, dims), out_shape=jax.ShapeDtypeS...  163 us

profile of v4, /device:TPU:26, one launch (start us, length us, event | category | flops | bytes accessed | tf_op | source)
XLA Modules:
  0.0 166.5 jit_solution(2036277818208213517)
XLA Ops:
  0.0 1.3 copy.8.taps
  1.3 163.3 %shard_map.73 = bf16[512,512]{1,0:T(8,128)(2,1)} custom-call(bf16[512,512]{1,0:T(8,128)(2,1)} %stream.1, f32[2,2048]{1,0:T(2,128)} %gain.1, bf16[2,256,512]{2,1,0:T(8,128)(2,1)} %w_value.1, bf16[2,256,512]{2,1,0:T(8,128)(2,1)} %w_inner.1, bf16[2,256,512]{2,1,0:T(8,128)(2,1)} %w_outer.1, f32[2,3,512]{2,1,0:T(4,128)} %copy.8.taps, bf16[2,512,256]{2,1,0:T(8,128)(2,1)} %w_output.1), custom_call_target="tpu_custom_call" | custom-call | tf_op jit(solution)/shard_map/pallas_call | solution.py:355
  164.6 1.9 %copy.10 = bf16[512,512]{1,0:T(8,128)(2,1)} copy(bf16[512,512]{1,0:T(8,128)(2,1)} %shard_map.73) | data formatting | bytes 1048576
